TPU v7x, 32 devices: a whole 2x2x4 slice. The times are simulated.
32 devices in a mesh: ep: 8 (over z, core), tp: 4 (over y, x).
Axes of the slice: x: 2, y: 2, z: 4, core: 2. Of those that a mesh axis runs over, the one named last changes fastest.
Arguments:
- q_latent: bfloat16 [4096, 512], P('ep'), may hold values from -6 to 6
- kv_latent: bfloat16 [4096, 256], P('ep'), may hold values from -6 to 6
- rope_key: bfloat16 [4096, 32], P('ep'), may hold values from -400 to 400
- q_gain: bfloat16 [512], replicated, may hold values from 0.099609375 to 1.8984375
- kv_gain: bfloat16 [256], replicated, may hold values from 0.099609375 to 1.8984375
- w_q_nope: bfloat16 [512, 1024], P(None, 'tp'), may hold values from -0.25 to 0.25
- w_q_rope: bfloat16 [512, 512], P(None, 'tp'), may hold values from -0.25 to 0.25
- w_k_nope: bfloat16 [256, 1024], P(None, 'tp'), may hold values from -0.375 to 0.375
- w_value: bfloat16 [256, 1024], P(None, 'tp'), may hold values from -0.375 to 0.375
- w_out: bfloat16 [1024, 2048], P('tp'), may hold values from -5.375 to 5.375
- tokens_b: bfloat16 [1024, 2048], P('ep'), may hold values from -6 to 6
- norm_gain_b: bfloat16 [2048], replicated, may hold values from 0.099609375 to 1.8984375
- routes: int32 [1024, 2], P('ep'), may hold values from 0 to 7, all different within a row; in each aligned block of 128 rows (0 to 127, 128 to 255, ...) at most 48 rows name the same one
- route_logits: float32 [1024, 2], P('ep'), may hold values from -6 to 6
- w_gate: bfloat16 [8, 2048, 4096], P('ep', None, 'tp'), may hold values from -0.125 to 0.125
- w_up: bfloat16 [8, 2048, 4096], P('ep', None, 'tp'), may hold values from -0.125 to 0.125
- w_down: bfloat16 [8, 4096, 2048], P('ep', 'tp'), may hold values from -0.125 to 0.125
Outputs:
- mixer_out: bfloat16 [4096, 2048], P(('ep', 'tp'))
- expert_mix: bfloat16 [1024, 2048], P('ep', 'tp')
Inputs may be any that keep to these rules, and one draw needn't show every extreme that they name: `routes`: each row names two different experts. In each aligned block of 128 rows (the rows of one index of ep) no expert is named by more than 48 rows, and in every draw some expert is named by exactly 48 rows of some block.
All inputs are finite; a program needn't handle non-finite values.
Results may differ from a plain program's by a relative error of at most 0.022.
The roundings to bfloat16 on the way count: a program that leaves them out, or rounds other values in their place, can miss the bound.
Values may be sent and summed in bfloat16 or wider, within the bound.
A program may use at most 128 MiB of HBM per device.

v0:
```python
import functools
import math

import jax
import jax.numpy as jnp
from jax import lax
from jax.experimental import pallas as pl
from jax.experimental.pallas import tpu as pltpu
from jax.sharding import PartitionSpec as P

NOPE = 64
ROPE = 32
VDIM = 64
LANES = 128
EPSILON = 1e-06
BF = jnp.bfloat16
F32 = jnp.float32


def rms_rows(values, gain):
    wide = values.astype(F32)
    scaled = wide * lax.rsqrt(jnp.mean(wide * wide, axis=-1, keepdims=True) + EPSILON)
    return (scaled * gain.astype(F32)).astype(BF)


def angle_tables(places):
    half = ROPE // 2
    freqs = 10000.0 ** (-jnp.arange(half, dtype=F32) / half)
    angles = places.astype(F32)[:, None] * freqs[None, :]
    return jnp.cos(angles), jnp.sin(angles)


MESH = pl.DeviceIdType.MESH


def remote(src, dst, send, recv, ep, tp):
    return pltpu.make_async_remote_copy(
        src_ref=src,
        dst_ref=dst,
        send_sem=send,
        recv_sem=recv,
        device_id={"ep": ep, "tp": tp},
        device_id_type=MESH,
    )


def loop(count, body, start=0):
    def step(i, c):
        body(i)
        return c

    lax.fori_loop(start, count, step, 0)


class Gather:
    def __init__(self, n_ep, n_tp, own, buf, local, recv, send_z, send_t, send_c):
        self.n_tp, self.nz = n_tp, n_ep // 2
        self.own, self.buf, self.local = own, buf, local
        self.square = n_tp == 4
        self.direct = 3 if self.square else n_tp
        self.recv, self.send_z, self.send_t, self.send_c = recv, send_z, send_t, send_c
        ep = lax.axis_index("ep")
        self.z, self.core, self.t = ep // 2, ep % 2, lax.axis_index("tp")
        self.ep = ep

    def slot(self, z, core, t):
        return (z * 2 + core) * self.n_tp + t

    def at_z(self, d):
        return (self.z + self.nz - d) % self.nz

    def at_t(self, d, back=True):
        if self.square:
            return (self.t // 2 + d // 2) % 2 * 2 + (self.t % 2 + d % 2) % 2
        return (self.t + (self.n_tp - d if back else d)) % self.n_tp

    def copy_z(self, d):
        me = self.slot(self.z, self.core, self.t)
        to = (self.z + d) % self.nz
        return remote(
            self.own, self.buf.at[me], self.send_z.at[d], self.recv.at[me], to * 2 + self.core, self.t
        )

    def copy_t(self, dz, d):
        s = self.slot(self.at_z(dz), self.core, self.t)
        to = self.at_t(d, False)
        return remote(
            self.buf.at[s], self.buf.at[s], self.send_t.at[dz * self.n_tp + d], self.recv.at[s], self.ep, to
        )

    def relay(self, dz):
        s = self.slot(self.at_z(dz), self.core, self.at_t(1 + dz % 2))
        to = self.at_t(2 - dz % 2)
        return remote(
            self.buf.at[s], self.buf.at[s], self.send_t.at[dz * self.n_tp + 3], self.recv.at[s], self.ep, to
        )

    def copy_c(self, dz, d):
        s = self.slot(self.at_z(dz), self.core, self.at_t(d))
        return remote(
            self.buf.at[s],
            self.buf.at[s],
            self.send_c.at[dz * self.n_tp + d],
            self.recv.at[s],
            self.z * 2 + 1 - self.core,
            self.t,
        )

    def landed(self, s):
        remote(self.own, self.buf.at[s], self.local, self.recv.at[s], self.ep, self.t).wait_recv()

    def start(self):
        loop(self.nz, lambda d: self.copy_z(d).start(), 1)
        me = self.slot(self.z, self.core, self.t)
        mine = pltpu.make_async_copy(self.own, self.buf.at[me], self.local)
        mine.start()
        mine.wait()

    def over_tp(self):
        def one(dz):
            @pl.when(dz > 0)
            def _():
                self.landed(self.slot(self.at_z(dz), self.core, self.t))

            loop(self.direct, lambda d: self.copy_t(dz, d).start(), 1)
            self.copy_c(dz, 0).start()

        loop(self.nz, one)

    def to_sibling(self):
        def one(dz):
            def inner(d):
                self.landed(self.slot(self.at_z(dz), self.core, self.at_t(d)))
                self.copy_c(dz, d).start()

            loop(self.direct, inner, 1)
            if self.square:
                self.relay(dz).start()

        loop(self.nz, one)

    def last(self):
        def one(dz):
            self.landed(self.slot(self.at_z(dz), self.core, self.at_t(3)))
            self.copy_c(dz, 3).start()

        if self.square:
            loop(self.nz, one)

    def finish(self):
        def one(dz):
            def inner(d):
                self.landed(self.slot(self.at_z(dz), 1 - self.core, self.at_t(d)))
                self.copy_c(dz, d).wait_send()

            loop(self.n_tp, inner)
            loop(self.direct, lambda d: self.copy_t(dz, d).wait_send(), 1)
            if self.square:
                self.relay(dz).wait_send()

        loop(self.nz, one)
        loop(self.nz, lambda d: self.copy_z(d).wait_send(), 1)


def greet(n_ep, n_tp, every_ep):
    ep, t = lax.axis_index("ep"), lax.axis_index("tp")
    barrier = pltpu.get_barrier_semaphore()

    def hello(e, tp):
        pl.semaphore_signal(barrier, inc=1, device_id={"ep": e, "tp": tp}, device_id_type=MESH)

    loop(n_tp, lambda d: hello(ep, (t + d) % n_tp), 1)
    if every_ep:
        loop(n_ep, lambda d: hello((ep + d) % n_ep, t), 1)
        pl.semaphore_wait(barrier, n_tp + n_ep - 2)
    else:
        nz = n_ep // 2
        loop(nz, lambda d: hello((ep // 2 + d) % nz * 2 + ep % 2, t), 1)
        hello(ep // 2 * 2 + 1 - ep % 2, t)
        pl.semaphore_wait(barrier, n_tp + nz - 1)


def attention_kernel(
    heads,
    n_ep,
    n_tp,
    sent_ref,
    tok_ref,
    lat_ref,
    gain_ref,
    cos_ref,
    sin_ref,
    qn_ref,
    qr_ref,
    wk_ref,
    wv_ref,
    out_ref,
    tok_out,
    kv_buf,
    k_buf,
    v_buf,
    q_ref,
    w_ref,
    *sems,
):
    part, lat = sent_ref.shape[0], wk_ref.shape[0]
    keys = n_ep * n_tp * part
    rows = lat_ref.shape[0]
    scale = (NOPE + ROPE) ** (-0.5) * math.log2(math.e)
    q_block = min(256, rows)
    k_block = 1024
    wide = heads * LANES
    latents = Gather(n_ep, n_tp, sent_ref, kv_buf, *sems[:5])
    tokens = Gather(n_ep, n_tp, tok_ref, tok_out, *sems[5:])
    greet(n_ep, n_tp, False)
    latents.start()
    latents.over_tp()
    tokens.start()

    def beside(parts, depth, width):
        filler = jnp.zeros((depth, LANES - width), BF)
        return jnp.concatenate(parts + [filler], axis=1)

    for h in range(heads):
        nope, value = slice(h * NOPE, (h + 1) * NOPE), slice(h * VDIM, (h + 1) * VDIM)
        w_ref[:, h * LANES : (h + 1) * LANES] = beside([wk_ref[:, nope]], lat, NOPE)
        w_ref[:, wide + h * LANES : wide + (h + 1) * LANES] = beside([wv_ref[:, value]], lat, VDIM)
    normed = rms_rows(lat_ref[...], gain_ref[...])
    deep, half = lat_ref.shape[1], ROPE // 2
    for h in range(heads):
        turn = qr_ref[:, h * ROPE : (h + 1) * ROPE]
        plain = beside([qn_ref[:, h * NOPE : (h + 1) * NOPE], turn], deep, NOPE + ROPE)
        blank = jnp.zeros((deep, NOPE), BF)
        turned = beside([blank, -turn[:, half:], turn[:, :half]], deep, NOPE + ROPE)
        q = jnp.dot(normed, plain, preferred_element_type=F32) * cos_ref[...]
        q = q + jnp.dot(normed, turned, preferred_element_type=F32) * sin_ref[...]
        q_ref[h] = q.astype(BF)
    latents.to_sibling()
    latents.last()
    latents.finish()
    tokens.over_tp()
    group = max(1, 512 // part)
    chunk = group * part

    def project(c):
        here = pl.ds(pl.multiple_of(c * chunk, chunk), chunk)
        block = kv_buf[pl.ds(c * group, group)].reshape(chunk, kv_buf.shape[2])
        up = jnp.dot(block[:, :lat], w_ref[...], preferred_element_type=F32)
        turned = block[:, lat:].astype(F32)
        lane = lax.broadcasted_iota(jnp.int32, (chunk, LANES), 1)
        for h in range(heads):
            k_buf[h, here, :] = (up[:, h * LANES : (h + 1) * LANES] + turned).astype(BF)
            v = up[:, wide + h * LANES : wide + (h + 1) * LANES]
            v_buf[h, here, :] = jnp.where(lane < VDIM, v, 1.0).astype(BF)

    loop(keys // chunk, project)

    def attend_head(h, here):
        q = q_ref[h, here, :]
        top, acc = None, None
        for j in range(keys // k_block):
            at = slice(j * k_block, (j + 1) * k_block)
            s = lax.dot_general(
                q, k_buf[h, at, :], (((1,), (1,)), ((), ())), preferred_element_type=F32
            )
            new_top = jnp.max(s, axis=-1, keepdims=True)
            if j > 0:
                new_top = jnp.maximum(top, new_top)
            p = jnp.exp2((s - new_top) * scale).astype(BF)
            pv = jnp.dot(p, v_buf[h, at, :], preferred_element_type=F32)
            acc = pv if j == 0 else acc * jnp.exp2((top - new_top) * scale) + pv
            top = new_top
        return (acc[:, :VDIM] / acc[:, VDIM : VDIM + 1]).astype(BF)

    def attend(step):
        here = pl.ds(pl.multiple_of(step * q_block, q_block), q_block)
        done = [attend_head(h, here) for h in range(heads)]
        out_ref[here, :] = done[0] if heads == 1 else jnp.concatenate(done, axis=1)

        @pl.when(step == max(rows // q_block // 2 - 1, 0))
        def _():
            tokens.to_sibling()

    loop(rows // q_block, attend)
    tokens.last()
    tokens.finish()


def gather_sems(n_ep, n_tp):
    dma = pltpu.SemaphoreType.DMA
    blocks = n_ep // 2 * n_tp
    return [dma, dma((n_ep * n_tp,)), dma((n_ep // 2,)), dma((blocks,)), dma((blocks,))]


def attention(n_ep, n_tp, heads, *operands):
    sent, tok, latent = operands[:3]
    rows = latent.shape[0]
    part = sent.shape[0]
    n = n_ep * n_tp
    keys = part * n
    flops = 4 * heads * rows * keys * 256
    vmem = pl.BlockSpec(memory_space=pltpu.VMEM)
    return pl.pallas_call(
        functools.partial(attention_kernel, heads, n_ep, n_tp),
        out_shape=(
            jax.ShapeDtypeStruct((rows, heads * VDIM), BF),
            jax.ShapeDtypeStruct((n,) + tok.shape, BF),
        ),
        in_specs=[vmem] * len(operands),
        out_specs=(vmem, vmem),
        scratch_shapes=[
            pltpu.VMEM((n,) + sent.shape, BF),
            pltpu.VMEM((heads, keys, LANES), BF),
            pltpu.VMEM((heads, keys, LANES), BF),
            pltpu.VMEM((heads, rows, LANES), BF),
            pltpu.VMEM((operands[-1].shape[0], 2 * heads * LANES), BF),
        ]
        + gather_sems(n_ep, n_tp)
        + gather_sems(n_ep, n_tp),
        compiler_params=pltpu.CompilerParams(
            vmem_limit_bytes=60 * 1024 * 1024, collective_id=0, has_side_effects=True
        ),
        cost_estimate=pl.CostEstimate(
            flops=flops, bytes_accessed=8 * 1024 * 1024, transcendentals=heads * rows * keys
        ),
        name="attention",
    )(*operands)


def experts_kernel(
    n_ep,
    n_tp,
    att_ref,
    wo_ref,
    pick_ref,
    scale_ref,
    own_ref,
    wg_hbm,
    wu_hbm,
    wd_hbm,
    tok_hbm,
    mix_ref,
    exp_ref,
    wg,
    wu,
    wd,
    tok,
    piece_ref,
    hid,
    p_send,
    p_recv,
    t_send,
    t_recv,
    e_send,
    e_recv,
    w_sem,
    ps,
    pr,
    ts,
    tr,
    es,
    er,
):
    ep, t = lax.axis_index("ep"), lax.axis_index("tp")
    part = mix_ref.shape[0]
    total, share = t_send.shape[1:]
    room = e_send.shape[1]
    loads = [
        pltpu.make_async_copy(a, b, w_sem.at[i])
        for i, (a, b) in enumerate(
            ((tok_hbm, tok), (wg_hbm, wg), (wu_hbm, wu), (wd_hbm, wd))
        )
    ]
    for load in loads:
        load.start()
    greet(n_ep, n_tp, True)

    def to_tp(send, recv, ss, rs, d):
        to = (t + d) % n_tp
        return remote(send.at[to], recv.at[t], ss.at[d], rs.at[t], ep, to)

    def from_tp(send, recv, ss, rs, d):
        frm = (t + n_tp - d) % n_tp
        remote(send.at[frm], recv.at[frm], ss.at[0], rs.at[frm], ep, frm).wait_recv()
        return frm

    mixer = (p_send, p_recv, ps, pr)
    terms = (t_send, t_recv, ts, tr)

    def project(d):
        to = (t + d) % n_tp
        rows = att_ref[pl.ds(pl.multiple_of(to * part, part), part), :]
        p_send[to] = jnp.dot(rows, wo_ref[...], preferred_element_type=F32).astype(BF)

        @pl.when(d < n_tp)
        def _():
            to_tp(*mixer, d).start()

    loop(n_tp + 1, project, 1)

    loads[0].wait()
    span = 512

    def select(c):
        at = pl.ds(pl.multiple_of(c * span, span), span)
        rows = jnp.dot(pick_ref[...], tok[:, at], preferred_element_type=F32)
        piece_ref[:, at] = rows.astype(BF)

    loop(piece_ref.shape[1] // span, select)
    step = 256
    loads[1].wait()
    loads[2].wait()

    def up(c):
        at = pl.ds(pl.multiple_of(c * step, step), step)
        g = jnp.dot(piece_ref[...], wg[:, at], preferred_element_type=F32)
        u = jnp.dot(piece_ref[...], wu[:, at], preferred_element_type=F32)
        hid[:, at] = (g / (1.0 + jnp.exp(-g)) * u).astype(BF)

    loop(hid.shape[1] // step, up)
    loads[3].wait()

    def down(d):
        to = (t + d) % n_tp
        at = pl.ds(pl.multiple_of(to * share, share), share)
        t_send[to] = jnp.dot(hid[...], wd[:, at], preferred_element_type=F32).astype(BF)

        @pl.when(d < n_tp)
        def _():
            to_tp(*terms, d).start()

    loop(n_tp + 1, down, 1)

    def reduced(send, group):
        acc = send[t].astype(F32)
        for d in range(1, n_tp):
            frm = from_tp(*group, d)
            acc = acc + group[1][frm].astype(F32)
        return acc

    mix_ref[...] = reduced(p_send, mixer).astype(BF)
    out = (reduced(t_send, terms) * scale_ref[:, :1]).astype(BF)
    e_send[...] = out.reshape(n_ep, room, share)
    e_recv[ep] = e_send[ep]

    def to_ep(d):
        to = (ep + d) % n_ep
        return remote(e_send.at[to], e_recv.at[ep], es.at[d], er.at[ep], to, t)

    loop(n_ep, lambda d: to_ep(d).start(), 1)

    def arrived(d):
        frm = (ep + n_ep - d) % n_ep
        remote(e_send.at[frm], e_recv.at[frm], es.at[0], er.at[frm], frm, t).wait_recv()

    loop(n_ep, arrived, 1)
    back = e_recv[...].reshape(n_ep * room, share)
    exp_ref[...] = jnp.dot(own_ref[...], back, preferred_element_type=F32).astype(BF)

    def drain(d):
        to_tp(*mixer, d).wait_send()
        to_tp(*terms, d).wait_send()

    loop(n_tp, drain, 1)
    loop(n_ep, lambda d: to_ep(d).wait_send(), 1)


def experts(n_ep, n_tp, room, att, w_out, pick, scale, own, w_gate, w_up, w_down, tok):
    vmem = pl.BlockSpec(memory_space=pltpu.VMEM)
    hbm = pl.BlockSpec(memory_space=pl.ANY)
    dma = pltpu.SemaphoreType.DMA
    width = w_out.shape[1]
    total = pick.shape[0]
    part, share = att.shape[0] // n_tp, width // n_tp
    flops = 6 * total * width * w_gate.shape[1] + 2 * att.shape[0] * att.shape[1] * width
    return pl.pallas_call(
        functools.partial(experts_kernel, n_ep, n_tp),
        out_shape=(
            jax.ShapeDtypeStruct((part, width), BF),
            jax.ShapeDtypeStruct((own.shape[0], share), BF),
        ),
        in_specs=[vmem] * 5 + [hbm] * 4,
        out_specs=(vmem, vmem),
        scratch_shapes=[
            pltpu.VMEM(w_gate.shape, BF),
            pltpu.VMEM(w_up.shape, BF),
            pltpu.VMEM(w_down.shape, BF),
            pltpu.VMEM(tok.shape, BF),
            pltpu.VMEM((total, width), BF),
            pltpu.VMEM((total, w_gate.shape[1]), BF),
            pltpu.VMEM((n_tp, part, width), BF),
            pltpu.VMEM((n_tp, part, width), BF),
            pltpu.VMEM((n_tp, total, share), BF),
            pltpu.VMEM((n_tp, total, share), BF),
            pltpu.VMEM((n_ep, room, share), BF),
            pltpu.VMEM((n_ep, room, share), BF),
            dma((4,)),
            dma((n_tp,)),
            dma((n_tp,)),
            dma((n_tp,)),
            dma((n_tp,)),
            dma((n_ep,)),
            dma((n_ep,)),
        ],
        compiler_params=pltpu.CompilerParams(
            vmem_limit_bytes=60 * 1024 * 1024, collective_id=1, has_side_effects=True
        ),
        cost_estimate=pl.CostEstimate(
            flops=flops, bytes_accessed=20 * 1024 * 1024, transcendentals=0
        ),
        name="experts",
    )(att, w_out, pick, scale, own, w_gate, w_up, w_down, tok)


def shards(
    q_latent,
    kv_latent,
    rope_key,
    q_gain,
    kv_gain,
    w_q_nope,
    w_q_rope,
    w_k_nope,
    w_value,
    w_out,
    tokens_b,
    norm_gain_b,
    routes,
    route_logits,
    w_gate,
    w_up,
    w_down,
):
    n_ep = lax.axis_size("ep")
    n_tp = lax.axis_size("tp")
    e_at = lax.axis_index("ep")
    t_at = lax.axis_index("tp")
    own_rows = q_latent.shape[0]
    heads = w_q_nope.shape[1] // NOPE
    rows_b = tokens_b.shape[0]
    width = tokens_b.shape[1]
    half = ROPE // 2

    part = own_rows // n_tp
    kv_part = lax.dynamic_slice_in_dim(kv_latent, t_at * part, part, 0)
    rope_part = lax.dynamic_slice_in_dim(rope_key, t_at * part, part, 0).astype(F32)
    places = e_at * own_rows + t_at * part + jnp.arange(part, dtype=jnp.int32)
    cosine, sine = angle_tables(places)
    first, second = rope_part[:, :half], rope_part[:, half:]
    sent = jnp.concatenate(
        [
            rms_rows(kv_part, kv_gain),
            jnp.zeros((part, NOPE), BF),
            (first * cosine - second * sine).astype(BF),
            (first * sine + second * cosine).astype(BF),
            jnp.zeros((part, LANES - NOPE - ROPE), BF),
        ],
        axis=1,
    )

    part_b = rows_b // n_tp
    tok_part = lax.dynamic_slice_in_dim(tokens_b, t_at * part_b, part_b, 0)
    route_part = lax.dynamic_slice_in_dim(routes, t_at * part_b, part_b, 0)
    logit_part = lax.dynamic_slice_in_dim(route_logits, t_at * part_b, part_b, 0)
    weights_b = jax.nn.softmax(logit_part, axis=-1)
    high = weights_b.astype(BF)
    low = (weights_b - high.astype(F32)).astype(BF)
    extra = jnp.concatenate(
        [route_part.astype(BF), high, low, jnp.zeros((part_b, LANES - 6), BF)], axis=1
    )
    sent_b = jnp.concatenate([rms_rows(tok_part, norm_gain_b), extra], axis=1)

    cos_q, sin_q = angle_tables(e_at * own_rows + jnp.arange(own_rows, dtype=jnp.int32))
    ones = jnp.ones((own_rows, NOPE), F32)
    tail = jnp.zeros((own_rows, LANES - NOPE - ROPE), F32)
    cos_row = jnp.concatenate([ones, cos_q, cos_q, tail], axis=1)
    sin_row = jnp.concatenate([0.0 * ones, sin_q, sin_q, tail], axis=1)
    attended, tok_all = attention(
        n_ep,
        n_tp,
        heads,
        sent,
        sent_b,
        q_latent,
        q_gain[None, :],
        cos_row,
        sin_row,
        w_q_nope,
        w_q_rope,
        w_k_nope,
        w_value,
    )
    tok_all = tok_all.reshape(n_ep * rows_b, width + LANES)

    room = -(-(3 * rows_b // n_ep) // 16) * 16
    total_b = tok_all.shape[0]
    info = tok_all[:, width : width + LANES].astype(F32)
    me = e_at.astype(F32)
    hit_0 = (info[:, 0] == me).astype(F32)
    hit_1 = (info[:, 1] == me).astype(F32)
    hit = hit_0 + hit_1
    weight = hit_0 * (info[:, 2] + info[:, 4]) + hit_1 * (info[:, 3] + info[:, 5])
    order = jnp.arange(rows_b)
    before = (order[:, None] < order[None, :]).astype(BF)
    slot = jnp.dot(hit.reshape(n_ep, rows_b).astype(BF), before, preferred_element_type=F32)
    row = slot + (jnp.arange(n_ep, dtype=F32) * room)[:, None]
    row = jnp.where(hit > 0, row.reshape(total_b), -1.0)
    index = jnp.arange(n_ep * room, dtype=F32)
    chosen = index[:, None] == row[None, :]
    pick = chosen.astype(BF)
    row_weight = jnp.sum(jnp.where(chosen, weight[None, :], 0.0), axis=1, keepdims=True)
    named = (routes[:, :, None] == jnp.arange(n_ep, dtype=jnp.int32)).astype(F32)
    used = jnp.sum(named, axis=1)
    ahead = jnp.dot(before.T, used.astype(BF), preferred_element_type=F32)
    own = (ahead[:, :, None] == jnp.arange(room, dtype=F32)) & (used[:, :, None] > 0)
    own = own.astype(BF).reshape(rows_b, n_ep * room)
    scale = jnp.broadcast_to(row_weight, (n_ep * room, LANES))
    mixer_out, expert_mix = experts(
        n_ep, n_tp, room, attended, w_out, pick, scale, own, w_gate[0], w_up[0], w_down[0], tok_all
    )
    return (mixer_out, expert_mix)


def solution(mesh):
    placed = (
        P("ep", None),
        P("ep", None),
        P("ep", None),
        P(),
        P(),
        P(None, "tp"),
        P(None, "tp"),
        P(None, "tp"),
        P(None, "tp"),
        P("tp", None),
        P("ep", None),
        P(),
        P("ep", None),
        P("ep", None),
        P("ep", None, "tp"),
        P("ep", None, "tp"),
        P("ep", "tp", None),
    )
    return jax.shard_map(
        shards,
        mesh=mesh,
        in_specs=placed,
        out_specs=(P(("ep", "tp"), None), P("ep", "tp")),
        check_vma=False,
    )
```

profile of v0, /device:TPU:0, one launch (start us, length us, event | category | flops | bytes accessed | tf_op | source)
XLA Modules:
  0.0 133.6 jit_solution(7104668325805554683)
XLA Ops:
  0.6 0.0 copy-start
  0.7 0.9 fusion.14
  1.6 1.0 fusion.10
  2.7 0.1 pad.7.clone
  2.8 0.7 convert_element_type.100
  3.5 0.7 constant_dynamic-slice_fusion.1
  4.2 0.8 fusion.31
  5.0 1.3 broadcast_in_dim.33.gain_ref
  6.3 0.7 convert_reduce_fusion
  7.0 0.1 fusion.25
  7.1 0.1 eq.88
  7.2 0.0 copy-done
  7.2 0.7 convert_element_type.107
  7.9 0.1 copy.45
  8.0 0.2 fusion.27
  8.2 0.1 subtract_convert_fusion
  8.3 0.1 copy.44
  8.4 0.1 copy.43
  8.5 0.3 fusion.24
  8.8 0.2 copy.42
  9.0 0.9 fusion.16
  10.0 0.8 concatenate.12.sent_ref
  10.7 1.0 fusion.12
  11.7 0.8 concatenate.13.tok_ref
  12.5 0.1 copy.41
  12.7 0.7 and_convert_fusion.own_ref
  13.3 1.0 multiply_sine_fusion
  14.3 1.1 maximum_maximum_fusion.1
  15.4 53.2 %attention.1 = (bf16[512,256]{1,0:T(8,128)(2,1)}, bf16[32,32,2176]{2,1,0:T(8,128)(2,1)}) custom-call(bf16[128,384]{1,0:T(8,128)(2,1)} %concatenate.12.sent_ref, bf16[32,2176]{1,0:T(8,128)(2,1)} %concatenate.13.tok_ref, bf16[512,512]{1,0:T(8,128)(2,1)} %lat_ref.1, bf16[1,512]{1,0:T(2,128)(2,1)} %broadcast_in_dim.33.gain_ref, ...), custom_call_target="tpu_custom_call" | custom-call | flops 8589934592 | bytes 8388608 | tf_op jit(solution)/shard_map/attention/pallas_call | solution.py:303
  68.6 1.0 slice_convert_fusion
  69.6 0.9 fusion.5
  70.5 0.2 fusion.9
  70.8 0.2 fusion.13
  71.0 0.1 fusion.2
  71.1 0.3 select_reduce_fusion
  71.4 0.8 broadcast_in_dim.39.scale_ref
  72.2 1.1 fusion.pick_ref
  73.3 56.8 %experts.1 = (bf16[128,2048]{1,0:T(8,128)(2,1)}, bf16[128,512]{1,0:T(8,128)(2,1)}) custom-call(bf16[512,256]{1,0:T(8,128)(2,1)} %get-tuple-element.4.att_ref, bf16[256,2048]{1,0:T(8,128)(2,1)} %wo_ref.1, bf16[384,1024]{1,0:T(8,128)(2,1)} %fusion.pick_ref, f32[384,128]{1,0:T(8,128)} %broadcast_in_dim.39.scale_ref, bf16[128,384]{1,0:T(8,128)(2,1)} %and_convert_fusion.own_ref, ...), custom_call_target="tpu_custom_call" | custom-call | flops 5368709120 | bytes 20971520 | tf_op jit(solution)/shard_map/experts/pallas_call | solution.py:476
  130.1 1.9 %copy.49 = bf16[128,2048]{1,0:T(8,128)(2,1)} copy(bf16[128,2048]{1,0:T(8,128)(2,1)} %get-tuple-element.21) | data formatting | bytes 1048576
  132.0 1.6 %copy.50 = bf16[128,512]{1,0:T(8,128)(2,1)} copy(bf16[128,512]{1,0:T(8,128)(2,1)} %get-tuple-element.22) | data formatting | bytes 262144
  (21 shorter events, 0.2 us)
Async XLA Ops:
  0.6 6.5 %copy-start = (bf16[512,32]{0,1:T(8,128)(2,1)S(1)}, bf16[512,32]{0,1:T(8,128)(2,1)}, u32[]{:S(2)}) copy-start(bf16[512,32]{0,1:T(8,128)(2,1)} %param.19) | copy-start | bytes 98308
where the time goes:
time: 134 us
  Pallas kernels  110 us (82%)
  other arithmetic  13.9 us (10%)
  local copies, waits for them, and re-layouts  8.6 us (6%)
    pallas_call x1, Pallas kernels, experts(): pl.pallas_call(functools.partial(experts_kernel, n_ep, n_tp), out_shape=(...  56.8 us
    pallas_call x1, Pallas kernels, attention(): pl.pallas_call(functools.partial(attention_kernel, heads, n_ep, n_tp), ou...  53.2 us
    unnamed x7, local copies, waits for them, and re-layouts  3.75 us
    convert_element_type x4, other arithmetic, rms_rows(): return (scaled * gain.astype(F32)).astype(BF)  3.28 us

commit v1 on v0

v1 whole, which is shorter than its diff:
```python
import functools
import math

import jax
import jax.numpy as jnp
import numpy as np
from jax import lax
from jax.experimental import pallas as pl
from jax.experimental.pallas import tpu as pltpu
from jax.sharding import PartitionSpec as P

NOPE = 64
ROPE = 32
VDIM = 64
LANES = 128
BAND = 16
EPSILON = 1e-06
BF = jnp.bfloat16
F32 = jnp.float32
MESH = pl.DeviceIdType.MESH


def rms_rows(values, gain):
    wide = values.astype(F32)
    scaled = wide * lax.rsqrt(jnp.mean(wide * wide, axis=-1, keepdims=True) + EPSILON)
    return (scaled * gain.astype(F32)).astype(BF)


def remote(src, dst, send, recv, ep, tp):
    return pltpu.make_async_remote_copy(
        src_ref=src,
        dst_ref=dst,
        send_sem=send,
        recv_sem=recv,
        device_id={"ep": ep, "tp": tp},
        device_id_type=MESH,
    )


def loop(count, body, start=0):
    def step(i, c):
        body(i)
        return c

    lax.fori_loop(start, count, step, 0)


class Spread:
    def __init__(self, count, n_tp, ep, t, view, index, recv, send, sib=None):
        self.count, self.n_tp, self.ep, self.t = count, n_tp, ep, t
        self.view, self.index, self.recv, self.send = view, index, recv, send
        self.square = n_tp == 4
        self.direct = 3 if self.square else n_tp
        self.sib = sib

    def at(self, d):
        if self.square:
            return (self.t // 2 + d // 2) % 2 * 2 + (self.t % 2 + d % 2) % 2
        return (self.t + d) % self.n_tp

    def frm(self, d):
        return self.at(d) if self.square else (self.t + self.n_tp - d) % self.n_tp

    def copy(self, i, d):
        ref = self.view(i, self.t)
        sem = self.recv.at[self.index(i, self.t)]
        return remote(ref, ref, self.send.at[i * self.n_tp + d], sem, self.ep, self.at(d))

    def passed(self, i):
        owner = self.at(1 + i % 2)
        ref = self.view(i, owner)
        sem = self.recv.at[self.index(i, owner)]
        return remote(ref, ref, self.send.at[i * self.n_tp + 3], sem, self.ep, self.at(2 - i % 2))

    def across(self, i, d):
        owner = self.frm(d)
        ref = self.view(i, owner)
        recv, send = self.sib
        sem = recv.at[self.index(i, owner)]
        return remote(ref, ref, send.at[i * self.n_tp + d], sem, self.ep // 2 * 2 + 1 - self.ep % 2, self.t)

    def landed(self, i, d):
        owner = self.frm(d)
        ref = self.view(i, owner)
        remote(ref, ref, self.send.at[0], self.recv.at[self.index(i, owner)], self.ep, self.t).wait_recv()

    def push(self, i):
        loop(self.direct, lambda d: self.copy(i, d).start(), 1)

    def relay(self, i):
        def one(d):
            self.landed(i, d)
            if self.sib is not None:
                self.across(i, d).start()

        loop(self.direct, one, 1)
        if self.square:
            self.passed(i).start()

    def last(self, i):
        if self.square:
            self.landed(i, 3)
            if self.sib is not None:
                self.across(i, 3).start()

    def drain(self, i, first=1):
        loop(self.direct, lambda d: self.copy(i, d).wait_send(), 1)
        if self.square:
            self.passed(i).wait_send()
        if self.sib is not None:
            loop(self.n_tp, lambda d: self.across(i, d).wait_send(), first)


def mega_kernel(
    heads,
    n_ep,
    n_tp,
    kv_ref,
    rope_ref,
    lat_ref,
    qg_ref,
    kvg_ref,
    bg_ref,
    cosb_ref,
    sinb_ref,
    cosa_ref,
    sina_ref,
    qn_ref,
    qr_ref,
    wk_ref,
    wv_ref,
    tokb_ref,
    route_ref,
    logit_ref,
    wo_hbm,
    wg_hbm,
    wu_hbm,
    wd_hbm,
    mix_ref,
    exp_ref,
    wo,
    wg,
    wu,
    wd,
    kv_buf,
    k_buf,
    v_buf,
    q_ref,
    w_ref,
    acc_ref,
    top_ref,
    att_ref,
    a_buf,
    x_send,
    x_recv,
    hid,
    t_send,
    t_recv,
    e_send,
    e_recv,
    own_hi,
    own_lo,
    w_sem,
    lat_zs,
    lat_ts,
    lat_cs,
    lat_recv,
    lat_own,
    x_zs,
    x_ts,
    x_recv_sem,
    x_own,
    wo_ts,
    wo_recv,
    wo_cs,
    wo_crecv,
    as_,
    ar,
    ts,
    tr,
    es,
    er,
):
    ep, t = lax.axis_index("ep"), lax.axis_index("tp")
    nz = n_ep // 2
    z, core = ep // 2, ep % 2
    sibling = z * 2 + 1 - core
    rows, deep = lat_ref.shape
    lat = wk_ref.shape[0]
    unit = kv_buf.shape[2]
    part = rows // n_tp
    room, width = x_send.shape[1:]
    share = width // n_tp
    rows_b = tokb_ref.shape[0]
    depth = wo.shape[1]
    pieces = wo_ts.shape[0] // n_tp
    slab = depth // 2 // pieces
    half = ROPE // 2
    scale = (NOPE + ROPE) ** (-0.5) * math.log2(math.e)
    wide = heads * LANES

    loads = [
        pltpu.make_async_copy(a, b, w_sem.at[i])
        for i, (a, b) in enumerate(((wo_hbm, wo.at[t]), (wg_hbm, wg), (wu_hbm, wu), (wd_hbm, wd)))
    ]
    for load in loads:
        load.start()

    barrier = pltpu.get_barrier_semaphore()

    def hello(e, tp):
        pl.semaphore_signal(barrier, inc=1, device_id={"ep": e, "tp": tp}, device_id_type=MESH)

    loop(n_tp, lambda d: hello(ep, (t + d) % n_tp), 1)
    loop(n_ep, lambda d: hello((ep + d) % n_ep, t), 1)

    def columns(s):
        return pl.ds(pl.multiple_of(s * share, share), share)

    def plane(d):
        return (z + d) % nz

    slots = n_ep * room
    lane = lax.broadcasted_iota(jnp.int32, (rows_b, slots), 1)
    expert = jnp.floor((lane.astype(F32) + 0.5) * (1.0 / room))
    place = lane.astype(F32) - expert * room
    first = route_ref[:, :1].astype(F32) == expert
    second = route_ref[:, 1:2].astype(F32) == expert
    named = (first | second).astype(F32)
    r = lax.broadcasted_iota(jnp.int32, (rows_b, rows_b), 0)
    c = lax.broadcasted_iota(jnp.int32, (rows_b, rows_b), 1)
    ahead = jnp.dot((c < r).astype(F32).astype(BF), named.astype(BF), preferred_element_type=F32)
    mine = jnp.where(ahead == place, named, 0.0)
    logits = logit_ref[...]
    peak = jnp.max(logits, axis=-1, keepdims=True)
    grown = jnp.exp(logits - peak)
    weights = grown / jnp.sum(grown, axis=-1, keepdims=True)
    weighted = mine * jnp.where(first, weights[:, :1], weights[:, 1:2])
    high = weighted.astype(BF)
    own_hi[...] = high
    own_lo[...] = (weighted - high.astype(F32)).astype(BF)

    normed_b = rms_rows(tokb_ref[...], bg_ref[...])
    pick = jnp.transpose(mine).astype(BF)
    span = min(512, width)
    for s in range(width // span):
        got = jnp.dot(pick, normed_b[:, s * span : (s + 1) * span], preferred_element_type=F32)
        x_send[:, :, s * span : (s + 1) * span] = got.astype(BF).reshape(n_ep, room, span)
    x_recv[ep] = x_send[ep]

    cos_a, sin_a = cosa_ref[pl.ds(ep, 1), :], sina_ref[pl.ds(ep, 1), :]
    cos = cos_a * cosb_ref[...] - sin_a * sinb_ref[...]
    sin = sin_a * cosb_ref[...] + cos_a * sinb_ref[...]
    normed_kv = rms_rows(kv_ref[...], kvg_ref[...])
    raw = rope_ref[...].astype(F32)
    front = jnp.zeros((rows, NOPE), F32)
    back = jnp.zeros((rows, LANES - NOPE - ROPE), F32)
    plain = jnp.concatenate([front, raw, back], axis=1)
    turned = jnp.concatenate([front, -raw[:, half:], raw[:, :half], back], axis=1)
    rot = plain * cos + turned * sin
    for s in range(n_tp):
        kv_buf[ep, s, :part, :] = normed_kv[s * part : (s + 1) * part]
        bands = [jnp.zeros((BAND, LANES), F32)] * ((unit - part) // BAND * 2)
        for g in range(part // BAND):
            at = s * part + g * BAND
            shift = (32 * (g % 4) - NOPE) % LANES
            piece = rot[at : at + BAND]
            bands[g // 4] = bands[g // 4] + (pltpu.roll(piece, shift, 1) if shift else piece)
        for b in range(len(bands) // 2):
            pair = jnp.concatenate(bands[2 * b : 2 * b + 2], axis=1).astype(BF)
            kv_buf[ep, s, part + b * BAND : part + (b + 1) * BAND, :] = pair

    pl.semaphore_wait(barrier, n_tp + n_ep - 2)

    def x_to(i):
        to = plane(1 + i // 2) * 2 + i % 2
        at = columns(t)
        return remote(
            x_send.at[to, :, at],
            x_recv.at[ep, :, at],
            x_zs.at[i],
            x_recv_sem.at[ep * n_tp + t],
            to,
            t,
        )

    def x_from(i):
        return plane(1 + i // 2) * 2 + i % 2

    routed = Spread(
        n_ep - 2,
        n_tp,
        ep,
        t,
        lambda i, s: x_recv.at[x_from(i), :, columns(s)],
        lambda i, s: x_from(i) * n_tp + s,
        x_recv_sem,
        x_ts,
    )
    x_beside = remote(x_send.at[sibling], x_recv.at[ep], x_own.at[0], x_own.at[1], sibling, t)

    def l_to(d):
        mine = kv_buf.at[ep, t]
        return remote(mine, mine, lat_zs.at[d], lat_recv.at[ep * n_tp + t], plane(d) * 2 + core, t)

    def l_from(i):
        return plane(1 + i) * 2 + core

    latents = Spread(
        nz - 1,
        n_tp,
        ep,
        t,
        lambda i, s: kv_buf.at[l_from(i), s],
        lambda i, s: l_from(i) * n_tp + s,
        lat_recv,
        lat_ts,
        (lat_recv, lat_cs),
    )
    l_beside = remote(kv_buf.at[ep], kv_buf.at[ep], lat_own.at[0], lat_own.at[1], sibling, t)

    projection = Spread(
        pieces,
        n_tp,
        ep,
        t,
        lambda i, s: wo.at[s, pl.ds(pl.multiple_of((core * pieces + i) * slab, slab), slab), :],
        lambda i, s: i * n_tp + s,
        wo_recv,
        wo_ts,
        (wo_crecv, wo_cs),
    )

    l_beside.start()
    x_beside.start()
    loop(n_ep - 2, lambda i: x_to(i).start())
    loop(nz, lambda d: l_to(d).start(), 1)
    loads[0].wait()
    projection.push(0)

    def beside(parts, height, filled):
        filler = jnp.zeros((height, LANES - filled), BF)
        return jnp.concatenate(parts + [filler], axis=1)

    for h in range(heads):
        nope, value = slice(h * NOPE, (h + 1) * NOPE), slice(h * VDIM, (h + 1) * VDIM)
        w_ref[:, h * LANES : (h + 1) * LANES] = beside([wk_ref[:, nope]], lat, NOPE)
        w_ref[:, wide + h * LANES : wide + (h + 1) * LANES] = beside([wv_ref[:, value]], lat, VDIM)
    normed = rms_rows(lat_ref[...], qg_ref[...])
    for h in range(heads):
        turn = qr_ref[:, h * ROPE : (h + 1) * ROPE]
        plain = beside([qn_ref[:, h * NOPE : (h + 1) * NOPE], turn], deep, NOPE + ROPE)
        blank = jnp.zeros((deep, NOPE), BF)
        turned = beside([blank, -turn[:, half:], turn[:, :half]], deep, NOPE + ROPE)
        q = jnp.dot(normed, plain, preferred_element_type=F32) * cos
        q = q + jnp.dot(normed, turned, preferred_element_type=F32) * sin
        q_ref[h] = q.astype(BF)

    keys = 2 * rows
    q_block = min(256, rows)

    def project(d):
        for j in range(2):
            block = kv_buf[plane(d) * 2 + j]
            tall = block[:, :part, :].reshape(rows, lat)
            up = jnp.dot(tall, w_ref[...], preferred_element_type=F32)
            pieces_ = []
            for s in range(n_tp):
                packed = block[s, part:, :].astype(F32)
                for g in range(part // BAND):
                    b, q = g // 8, g % 8 // 4
                    piece = packed[b * BAND : (b + 1) * BAND, q * LANES : (q + 1) * LANES]
                    shift = (NOPE - 32 * (g % 4)) % LANES
                    pieces_.append(pltpu.roll(piece, shift, 1) if shift else piece)
            turned = jnp.concatenate(pieces_, axis=0)
            spot = lax.broadcasted_iota(jnp.int32, (rows, LANES), 1)
            turned = jnp.where((spot >= NOPE) & (spot < NOPE + ROPE), turned, 0.0)
            at = slice(j * rows, (j + 1) * rows)
            for h in range(heads):
                k_buf[h, at, :] = (up[:, h * LANES : (h + 1) * LANES] + turned).astype(BF)
                v = up[:, wide + h * LANES : wide + (h + 1) * LANES]
                v_buf[h, at, :] = jnp.where(spot < VDIM, v, 1.0).astype(BF)

    def attend(h, step, start):
        here = pl.ds(step * q_block if isinstance(step, int) else pl.multiple_of(step * q_block, q_block), q_block)
        s = lax.dot_general(
            q_ref[h, here, :], k_buf[h], (((1,), (1,)), ((), ())), preferred_element_type=F32
        )
        top = jnp.max(s, axis=-1, keepdims=True)
        if not start:
            old = top_ref[h, here, :1]
            top = jnp.maximum(old, top)
        p = jnp.exp2((s - top) * scale).astype(BF)
        pv = jnp.dot(p, v_buf[h], preferred_element_type=F32)
        if not start:
            pv = acc_ref[h, here, :] * jnp.exp2((old - top) * scale) + pv
        acc_ref[h, here, :] = pv
        top_ref[h, here, :] = jnp.broadcast_to(top, (q_block, LANES))

    def attend_all(start):
        def step(i):
            for h in range(heads):
                attend(h, i, start)

        loop(rows // q_block, step)

    l_beside.wait_recv()
    project(0)
    attend_all(True)
    loop(n_ep - 2, lambda i: (routed.landed(i, 0), routed.push(i)))
    loop(nz - 1, lambda i: (latents.landed(i, 0), latents.push(i), latents.across(i, 0).start()))
    loop(n_ep - 2, routed.relay)
    loop(nz - 1, latents.relay)
    loop(pieces, projection.push, 1)
    x_beside.wait_recv()
    loop(n_ep - 2, routed.last)

    step = min(256, hid.shape[1])
    loads[1].wait()
    loads[2].wait()
    total = n_ep * room

    def up(i):
        at = pl.ds(pl.multiple_of(i * step, step), step)
        x = x_recv[...].reshape(total, width)
        g = jnp.dot(x, wg[:, at], preferred_element_type=F32)
        u = jnp.dot(x, wu[:, at], preferred_element_type=F32)
        hid[:, at] = (g / (1.0 + jnp.exp(-g)) * u).astype(BF)

    loop(hid.shape[1] // step, up)
    loads[3].wait()
    loop(nz - 1, latents.last)

    def to_tp(src, recv, ss, rs, d):
        return remote(src, recv.at[t], ss.at[d], rs.at[t], ep, (t + d) % n_tp)

    def from_tp(recv, ss, rs, d):
        frm = (t + n_tp - d) % n_tp
        remote(recv.at[frm], recv.at[frm], ss.at[0], rs.at[frm], ep, frm).wait_recv()
        return frm

    def term(d):
        return to_tp(t_send.at[(t + d) % n_tp], t_recv, ts, tr, d)

    def down(d):
        to = (t + d) % n_tp
        t_send[to] = jnp.dot(hid[...], wd[:, columns(to)], preferred_element_type=F32).astype(BF)

        @pl.when(d < n_tp)
        def _():
            term(d).start()

    loop(n_tp + 1, down, 1)

    def other(i):
        def beside_landed(s):
            at = plane(1 + i) * 2 + 1 - core
            ref = kv_buf.at[at, s]
            remote(ref, ref, lat_own.at[0], lat_recv.at[at * n_tp + s], sibling, t).wait_recv()

        loop(n_tp, beside_landed)
        project(1 + i)
        attend_all(False)

    def to_ep(d):
        to = (ep + d) % n_ep
        return remote(e_send.at[to], e_recv.at[ep], es.at[d], er.at[ep], to, t)

    def give_back():
        out = t_send[t].astype(F32)
        for d in range(1, n_tp):
            out = out + t_recv[from_tp(t_recv, ts, tr, d)].astype(F32)
        e_send[...] = out.astype(BF).reshape(n_ep, room, share)
        e_recv[ep] = e_send[ep]
        loop(n_ep, lambda d: to_ep(d).start(), 1)

    def tail(i):
        other(i)

        @pl.when(i == 0)
        def _():
            loop(pieces, projection.relay)

    loop(nz - 1, tail)
    loop(pieces, projection.last)

    def finish(i):
        here = pl.ds(pl.multiple_of(i * q_block, q_block), q_block)
        done = []
        for h in range(heads):
            acc = acc_ref[h, here, :]
            done.append((acc[:, :VDIM] / acc[:, VDIM : VDIM + 1]).astype(BF))
        att_ref[here, :] = done[0] if heads == 1 else jnp.concatenate(done, axis=1)

    loop(rows // q_block, finish)

    def piece_of(s):
        return pl.ds(pl.multiple_of(s * part, part), part)

    def attended(d):
        return to_tp(att_ref.at[piece_of((t + d) % n_tp), :], a_buf, as_, ar, d)

    loop(n_tp, lambda d: attended(d).start(), 1)
    a_buf[t] = att_ref[piece_of(t), :]
    give_back()

    def across_landed(i):
        def one(d):
            owner = projection.frm(d)
            at = pl.ds(pl.multiple_of(((1 - core) * pieces + i) * slab, slab), slab)
            ref = wo.at[owner, at, :]
            remote(ref, ref, wo_cs.at[0], wo_crecv.at[i * n_tp + owner], sibling, t).wait_recv()

        loop(n_tp, one, 1)

    loop(pieces, across_landed)
    for d in range(1, n_tp):
        from_tp(a_buf, as_, ar, d)

    def mix(s):
        at = pl.ds(pl.multiple_of(s * span, span), span)
        out = jnp.zeros((part, span), F32)
        for g in range(n_tp):
            out = out + jnp.dot(a_buf[g], wo[g, :, at], preferred_element_type=F32)
        mix_ref[:, at] = out.astype(BF)

    loop(width // span, mix)

    def arrived(d):
        frm = (ep + n_ep - d) % n_ep
        remote(e_recv.at[frm], e_recv.at[frm], es.at[0], er.at[frm], frm, t).wait_recv()

    loop(n_ep, arrived, 1)
    home = e_recv[...].reshape(total, share)
    out = jnp.dot(own_hi[...], home, preferred_element_type=F32)
    out = out + jnp.dot(own_lo[...], home, preferred_element_type=F32)
    exp_ref[...] = out.astype(BF)

    l_beside.wait_send()
    x_beside.wait_send()
    loop(n_ep - 2, lambda i: (x_to(i).wait_send(), routed.drain(i)))
    loop(nz, lambda d: l_to(d).wait_send(), 1)
    loop(nz - 1, lambda i: latents.drain(i, 0))
    loop(pieces, projection.drain)
    loop(n_tp, lambda d: (term(d).wait_send(), attended(d).wait_send()), 1)
    loop(n_ep, lambda d: to_ep(d).wait_send(), 1)


def turn_tables(n_ep, rows):
    half = ROPE // 2
    freqs = 10000.0 ** (-np.arange(half) / half)
    lanes = np.zeros(LANES)
    lanes[NOPE : NOPE + half] = freqs
    lanes[NOPE + half : NOPE + ROPE] = freqs
    near = np.arange(rows)[:, None] * lanes
    far = (np.arange(n_ep) * rows)[:, None] * lanes
    return [f(a).astype(np.float32) for a in (near, far) for f in (np.cos, np.sin)]


def mega(n_ep, n_tp, heads, operands, w_out, w_gate, w_up, w_down):
    kv, rope, latent = operands[:3]
    tokens = operands[14]
    rows = latent.shape[0]
    rows_b, width = tokens.shape
    lat = kv.shape[1]
    part = rows // n_tp
    unit = part + -(-part // LANES) * BAND
    room = -(-(3 * rows_b // n_ep) // BAND) * BAND
    total = n_ep * room
    share = width // n_tp
    hidden = w_gate.shape[1]
    nz = n_ep // 2
    depth = w_out.shape[0]
    pieces = min(4, depth // 2 // BAND)
    vmem = pl.BlockSpec(memory_space=pltpu.VMEM)
    hbm = pl.BlockSpec(memory_space=pl.ANY)
    dma = pltpu.SemaphoreType.DMA
    keys = rows * n_ep
    flops = 4 * heads * rows * keys * 256 + 6 * total * width * hidden
    return pl.pallas_call(
        functools.partial(mega_kernel, heads, n_ep, n_tp),
        out_shape=(
            jax.ShapeDtypeStruct((part, width), BF),
            jax.ShapeDtypeStruct((rows_b, share), BF),
        ),
        in_specs=[vmem] * len(operands) + [hbm] * 4,
        out_specs=(vmem, vmem),
        scratch_shapes=[
            pltpu.VMEM((n_tp,) + w_out.shape, BF),
            pltpu.VMEM(w_gate.shape, BF),
            pltpu.VMEM(w_up.shape, BF),
            pltpu.VMEM(w_down.shape, BF),
            pltpu.VMEM((n_ep, n_tp, unit, lat), BF),
            pltpu.VMEM((heads, 2 * rows, LANES), BF),
            pltpu.VMEM((heads, 2 * rows, LANES), BF),
            pltpu.VMEM((heads, rows, LANES), BF),
            pltpu.VMEM((lat, 2 * heads * LANES), BF),
            pltpu.VMEM((heads, rows, LANES), F32),
            pltpu.VMEM((heads, rows, LANES), F32),
            pltpu.VMEM((rows, heads * VDIM), BF),
            pltpu.VMEM((n_tp, part, heads * VDIM), BF),
            pltpu.VMEM((n_ep, room, width), BF),
            pltpu.VMEM((n_ep, room, width), BF),
            pltpu.VMEM((total, hidden), BF),
            pltpu.VMEM((n_tp, total, share), BF),
            pltpu.VMEM((n_tp, total, share), BF),
            pltpu.VMEM((n_ep, room, share), BF),
            pltpu.VMEM((n_ep, room, share), BF),
            pltpu.VMEM((rows_b, total), BF),
            pltpu.VMEM((rows_b, total), BF),
            dma((4,)),
            dma((nz,)),
            dma((nz * n_tp,)),
            dma((nz * n_tp,)),
            dma((n_ep * n_tp,)),
            dma((2,)),
            dma((n_ep,)),
            dma((n_ep * n_tp,)),
            dma((n_ep * n_tp,)),
            dma((2,)),
            dma((pieces * n_tp,)),
            dma((pieces * n_tp,)),
            dma((pieces * n_tp,)),
            dma((pieces * n_tp,)),
            dma((n_tp,)),
            dma((n_tp,)),
            dma((n_tp,)),
            dma((n_tp,)),
            dma((n_ep,)),
            dma((n_ep,)),
        ],
        compiler_params=pltpu.CompilerParams(
            vmem_limit_bytes=60 * 1024 * 1024, collective_id=0, has_side_effects=True
        ),
        cost_estimate=pl.CostEstimate(
            flops=flops, bytes_accessed=20 * 1024 * 1024, transcendentals=heads * rows * keys
        ),
        name="mega",
    )(*operands, w_out, w_gate, w_up, w_down)


def shards(
    q_latent,
    kv_latent,
    rope_key,
    q_gain,
    kv_gain,
    w_q_nope,
    w_q_rope,
    w_k_nope,
    w_value,
    w_out,
    tokens_b,
    norm_gain_b,
    routes,
    route_logits,
    w_gate,
    w_up,
    w_down,
):
    n_ep = lax.axis_size("ep")
    n_tp = lax.axis_size("tp")
    heads = w_q_nope.shape[1] // NOPE
    cos_b, sin_b, cos_a, sin_a = turn_tables(n_ep, q_latent.shape[0])
    operands = (
        kv_latent,
        rope_key,
        q_latent,
        q_gain[None, :],
        kv_gain[None, :],
        norm_gain_b[None, :],
        cos_b,
        sin_b,
        cos_a,
        sin_a,
        w_q_nope,
        w_q_rope,
        w_k_nope,
        w_value,
        tokens_b,
        routes,
        route_logits,
    )
    return mega(n_ep, n_tp, heads, operands, w_out, w_gate[0], w_up[0], w_down[0])


def solution(mesh):
    placed = (
        P("ep", None),
        P("ep", None),
        P("ep", None),
        P(),
        P(),
        P(None, "tp"),
        P(None, "tp"),
        P(None, "tp"),
        P(None, "tp"),
        P("tp", None),
        P("ep", None),
        P(),
        P("ep", None),
        P("ep", None),
        P("ep", None, "tp"),
        P("ep", None, "tp"),
        P("ep", "tp", None),
    )
    return jax.shard_map(
        shards,
        mesh=mesh,
        in_specs=placed,
        out_specs=(P(("ep", "tp"), None), P("ep", "tp")),
        check_vma=False,
    )
```

time: 134 us -> 91.8 us (0.69)
  Pallas kernels: 110 us -> 78.7 us
  other arithmetic: 13.9 us -> 0 us
  local copies, waits for them, and re-layouts: 8.6 us -> 11.6 us
    pallas_call x2 -> x1, Pallas kernels: 110 us -> 78.7 us  [mega(): pl.pallas_call(functools.partial(mega_kernel, heads, n_ep, n_tp), out_sha...]
    convert_element_type x14 -> x0, other arithmetic: 6.71 us -> none  [the longest x4 3.28 us: rms_rows(): return (scaled * gain.astype(F32)).astype(BF)]
    unnamed x7 -> x5, local copies, waits for them, and re-layouts: 3.75 us -> 7.78 us
    reduce_sum x5 -> x0, other arithmetic: 3.19 us -> none  [the longest x2 1.99 us: rms_rows(): jnp.mean(wide * wide, axis=-1, keepdims=True) + EPSILON]
    broadcast_in_dim x6 -> x2, local copies, waits for them, and re-layouts: 0.82 us -> 2.53 us  [the longest x1 1.29 us: shards(): norm_gain_b[None, :]]
    concatenate x5 -> x0, local copies, waits for them, and re-layouts: 1.6 us -> none  [the longest x1 0.76 us: shards(): sent_b = jnp.concatenate([rms_rows(tok_part, norm_gain_b), extra], axis=1)]
where the time goes in v1:
time: 91.8 us; the launch traced here: 90.9 us
  Pallas kernels  78.7 us (86%)
  local copies, waits for them, and re-layouts  11.6 us (13%)
    pallas_call x1, Pallas kernels, mega(): pl.pallas_call(functools.partial(mega_kernel, heads, n_ep, n_tp), out_sha...  78.7 us
    unnamed x5, local copies, waits for them, and re-layouts  7.78 us

profile of v1, /device:TPU:0, one launch (start us, length us, event | category | flops | bytes accessed | tf_op | source)
XLA Modules:
  0.0 90.9 jit_solution(11636989859811341720)
XLA Ops:
  0.6 1.2 %broadcast_in_dim.10.kvg_ref = bf16[1,256]{1,0:T(2,128)(2,1)} reshape(bf16[256]{0:T(256)(128)(2,1)} %param.25) | data formatting | bytes 1024 | tf_op jit(solution)/shard_map/broadcast_in_dim | solution.py:670
  1.9 1.3 %broadcast_in_dim.9.qg_ref = bf16[1,512]{1,0:T(2,128)(2,1)} reshape(bf16[512]{0:T(512)(128)(2,1)} %param.24) | data formatting | bytes 2048 | tf_op jit(solution)/shard_map/broadcast_in_dim | solution.py:669
  3.1 1.3 %broadcast_in_dim.11.bg_ref = bf16[1,2048]{1,0:T(2,128)(2,1)} reshape(bf16[2048]{0:T(1024)(128)(2,1)} %param.32) | data formatting | bytes 8192 | tf_op jit(solution)/shard_map/broadcast_in_dim | solution.py:671
  4.4 1.4 %copy.24.route_ref = s32[128,2]{1,0:T(8,128)} copy(s32[128,2]{0,1:T(2,128)} %param.33) | data formatting | bytes 2048 | tf_op args[12]
  5.8 1.4 %copy.25.logit_ref = f32[128,2]{1,0:T(8,128)} copy(f32[128,2]{0,1:T(2,128)} %param.34) | data formatting | bytes 2048 | tf_op args[13]
  7.2 1.5 %copy.23.rope_ref = bf16[512,32]{1,0:T(8,128)(2,1)} copy(bf16[512,32]{0,1:T(8,128)(2,1)} %param.23) | data formatting | bytes 65536 | tf_op args[2]
  8.7 78.7 %mega.1 = (bf16[128,2048]{1,0:T(8,128)(2,1)}, bf16[128,512]{1,0:T(8,128)(2,1)}) custom-call(bf16[512,256]{1,0:T(8,128)(2,1)} %kv_ref.1, bf16[512,32]{1,0:T(8,128)(2,1)} %copy.23.rope_ref, bf16[512,512]{1,0:T(8,128)(2,1)} %lat_ref.1, bf16[1,512]{1,0:T(2,128)(2,1)} %broadcast_in_dim.9.qg_ref, bf16[1,256]{1,0:T(2,128)(2,1)} %broadcast_in_dim.10.kvg_ref, ...), custom_call_target="tpu_custom_call" | custom-call | flops 13421772800 | bytes 20971520 | tf_op jit(solution)/shard_map/mega/pallas_call | solution.py:580
  87.4 1.9 %copy.28 = bf16[128,2048]{1,0:T(8,128)(2,1)} copy(bf16[128,2048]{1,0:T(8,128)(2,1)} %get-tuple-element.4) | data formatting | bytes 1048576
  89.3 1.6 %copy.29 = bf16[128,512]{1,0:T(8,128)(2,1)} copy(bf16[128,512]{1,0:T(8,128)(2,1)} %get-tuple-element.5) | data formatting | bytes 262144

commit v2 on v1

--- a/solution.py
+++ b/solution.py
@@ -118,9 +118,7 @@
     kv_ref,
     rope_ref,
     lat_ref,
-    qg_ref,
-    kvg_ref,
-    bg_ref,
+    gain_ref,
     cosb_ref,
     sinb_ref,
     cosa_ref,
@@ -220,27 +218,35 @@
     def plane(d):
         return (z + d) % nz
 
+    def source(d):
+        return (z + nz - d) % nz
+
     slots = n_ep * room
     lane = lax.broadcasted_iota(jnp.int32, (rows_b, slots), 1)
     expert = jnp.floor((lane.astype(F32) + 0.5) * (1.0 / room))
     place = lane.astype(F32) - expert * room
-    first = route_ref[:, :1].astype(F32) == expert
-    second = route_ref[:, 1:2].astype(F32) == expert
+    def standing(ref):
+        return jnp.transpose(jnp.broadcast_to(ref[:1, :], (8, rows_b))), jnp.transpose(
+            jnp.broadcast_to(ref[1:2, :], (8, rows_b))
+        )
+
+    route = [x[:, :1] for x in standing(route_ref[...].astype(F32))]
+    first, second = route[0] == expert, route[1] == expert
     named = (first | second).astype(F32)
     r = lax.broadcasted_iota(jnp.int32, (rows_b, rows_b), 0)
     c = lax.broadcasted_iota(jnp.int32, (rows_b, rows_b), 1)
     ahead = jnp.dot((c < r).astype(F32).astype(BF), named.astype(BF), preferred_element_type=F32)
     mine = jnp.where(ahead == place, named, 0.0)
     logits = logit_ref[...]
-    peak = jnp.max(logits, axis=-1, keepdims=True)
+    peak = jnp.max(logits, axis=0, keepdims=True)
     grown = jnp.exp(logits - peak)
-    weights = grown / jnp.sum(grown, axis=-1, keepdims=True)
-    weighted = mine * jnp.where(first, weights[:, :1], weights[:, 1:2])
+    weights = [x[:, :1] for x in standing(grown / jnp.sum(grown, axis=0, keepdims=True))]
+    weighted = mine * jnp.where(first, weights[0], weights[1])
     high = weighted.astype(BF)
     own_hi[...] = high
     own_lo[...] = (weighted - high.astype(F32)).astype(BF)
 
-    normed_b = rms_rows(tokb_ref[...], bg_ref[...])
+    normed_b = rms_rows(tokb_ref[...], gain_ref[:, deep + lat :])
     pick = jnp.transpose(mine).astype(BF)
     span = min(512, width)
     for s in range(width // span):
@@ -251,8 +257,8 @@
     cos_a, sin_a = cosa_ref[pl.ds(ep, 1), :], sina_ref[pl.ds(ep, 1), :]
     cos = cos_a * cosb_ref[...] - sin_a * sinb_ref[...]
     sin = sin_a * cosb_ref[...] + cos_a * sinb_ref[...]
-    normed_kv = rms_rows(kv_ref[...], kvg_ref[...])
-    raw = rope_ref[...].astype(F32)
+    normed_kv = rms_rows(kv_ref[...], gain_ref[:, deep : deep + lat])
+    raw = jnp.transpose(rope_ref[...].astype(F32))
     front = jnp.zeros((rows, NOPE), F32)
     back = jnp.zeros((rows, LANES - NOPE - ROPE), F32)
     plain = jnp.concatenate([front, raw, back], axis=1)
@@ -285,7 +291,7 @@
         )
 
     def x_from(i):
-        return plane(1 + i // 2) * 2 + i % 2
+        return source(1 + i // 2) * 2 + i % 2
 
     routed = Spread(
         n_ep - 2,
@@ -304,7 +310,7 @@
         return remote(mine, mine, lat_zs.at[d], lat_recv.at[ep * n_tp + t], plane(d) * 2 + core, t)
 
     def l_from(i):
-        return plane(1 + i) * 2 + core
+        return source(1 + i) * 2 + core
 
     latents = Spread(
         nz - 1,
@@ -346,7 +352,7 @@
         nope, value = slice(h * NOPE, (h + 1) * NOPE), slice(h * VDIM, (h + 1) * VDIM)
         w_ref[:, h * LANES : (h + 1) * LANES] = beside([wk_ref[:, nope]], lat, NOPE)
         w_ref[:, wide + h * LANES : wide + (h + 1) * LANES] = beside([wv_ref[:, value]], lat, VDIM)
-    normed = rms_rows(lat_ref[...], qg_ref[...])
+    normed = rms_rows(lat_ref[...], gain_ref[:, :deep])
     for h in range(heads):
         turn = qr_ref[:, h * ROPE : (h + 1) * ROPE]
         plain = beside([qn_ref[:, h * NOPE : (h + 1) * NOPE], turn], deep, NOPE + ROPE)
@@ -361,7 +367,7 @@
 
     def project(d):
         for j in range(2):
-            block = kv_buf[plane(d) * 2 + j]
+            block = kv_buf[source(d) * 2 + j]
             tall = block[:, :part, :].reshape(rows, lat)
             up = jnp.dot(tall, w_ref[...], preferred_element_type=F32)
             pieces_ = []
@@ -381,44 +387,31 @@
                 v = up[:, wide + h * LANES : wide + (h + 1) * LANES]
                 v_buf[h, at, :] = jnp.where(spot < VDIM, v, 1.0).astype(BF)
 
-    def attend(h, step, start):
-        here = pl.ds(step * q_block if isinstance(step, int) else pl.multiple_of(step * q_block, q_block), q_block)
+    def attend(h, here):
         s = lax.dot_general(
             q_ref[h, here, :], k_buf[h], (((1,), (1,)), ((), ())), preferred_element_type=F32
         )
-        top = jnp.max(s, axis=-1, keepdims=True)
-        if not start:
-            old = top_ref[h, here, :1]
-            top = jnp.maximum(old, top)
+        old = top_ref[h, here, :1]
+        top = jnp.maximum(old, jnp.max(s, axis=-1, keepdims=True))
         p = jnp.exp2((s - top) * scale).astype(BF)
         pv = jnp.dot(p, v_buf[h], preferred_element_type=F32)
-        if not start:
-            pv = acc_ref[h, here, :] * jnp.exp2((old - top) * scale) + pv
-        acc_ref[h, here, :] = pv
+        acc_ref[h, here, :] = acc_ref[h, here, :] * jnp.exp2((old - top) * scale) + pv
         top_ref[h, here, :] = jnp.broadcast_to(top, (q_block, LANES))
 
-    def attend_all(start):
-        def step(i):
-            for h in range(heads):
-                attend(h, i, start)
-
-        loop(rows // q_block, step)
-
-    l_beside.wait_recv()
-    project(0)
-    attend_all(True)
-    loop(n_ep - 2, lambda i: (routed.landed(i, 0), routed.push(i)))
-    loop(nz - 1, lambda i: (latents.landed(i, 0), latents.push(i), latents.across(i, 0).start()))
-    loop(n_ep - 2, routed.relay)
-    loop(nz - 1, latents.relay)
-    loop(pieces, projection.push, 1)
-    x_beside.wait_recv()
-    loop(n_ep - 2, routed.last)
-
+    together = min(2, heads)
+    beats = rows // q_block * heads // together
+
+    def beat(i):
+        at = i // (heads // together)
+        here = pl.ds(pl.multiple_of(at * q_block, q_block), q_block)
+        for h in range(together):
+            attend(i % (heads // together) * together + h, here)
+
+    top_ref[...] = jnp.full(top_ref.shape, -jnp.inf, F32)
+    acc_ref[...] = jnp.zeros(acc_ref.shape, F32)
+
+    total = n_ep * room
     step = min(256, hid.shape[1])
-    loads[1].wait()
-    loads[2].wait()
-    total = n_ep * room
 
     def up(i):
         at = pl.ds(pl.multiple_of(i * step, step), step)
@@ -427,10 +420,6 @@
         u = jnp.dot(x, wu[:, at], preferred_element_type=F32)
         hid[:, at] = (g / (1.0 + jnp.exp(-g)) * u).astype(BF)
 
-    loop(hid.shape[1] // step, up)
-    loads[3].wait()
-    loop(nz - 1, latents.last)
-
     def to_tp(src, recv, ss, rs, d):
         return remote(src, recv.at[t], ss.at[d], rs.at[t], ep, (t + d) % n_tp)
 
@@ -439,8 +428,27 @@
         remote(recv.at[frm], recv.at[frm], ss.at[0], rs.at[frm], ep, frm).wait_recv()
         return frm
 
+    def to_ep(d):
+        to = (ep + d) % n_ep
+        return remote(e_send.at[to], e_recv.at[ep], es.at[d], er.at[ep], to, t)
+
+    square = n_tp == 4
+    part_w = share // 2
+    xn, yn, dn = routed.at(1), routed.at(2), routed.at(3 if square else 1)
+    plan = [(dn, 0, xn, 0), (dn, 1, yn, 1), (xn, 0, xn, 2), (yn, 1, yn, 3)]
+    kept = [(yn, 0, yn, 4), (xn, 1, xn, 5), (t, 0, None, 6), (t, 1, None, 7)]
+
+    def hop(k):
+        to = (plan + kept)[k][2]
+        return remote(t_send.at[k], t_recv.at[k], ts.at[k], tr.at[k], ep, to)
+
     def term(d):
         return to_tp(t_send.at[(t + d) % n_tp], t_recv, ts, tr, d)
+
+    def summed_columns(k):
+        group, part_at = (plan + kept)[k][:2]
+        at = pl.ds(pl.multiple_of(group * share + part_at * part_w, part_w), part_w)
+        t_send[k] = jnp.dot(hid[...], wd[:, at], preferred_element_type=F32).astype(BF)
 
     def down(d):
         to = (t + d) % n_tp
@@ -450,39 +458,135 @@
         def _():
             term(d).start()
 
-    loop(n_tp + 1, down, 1)
-
-    def other(i):
+    def experts_up():
+        loads[1].wait()
+        loads[2].wait()
+        loop(hid.shape[1] // step, up)
+        loads[3].wait()
+
+    def experts_down():
+        if square:
+            for k in range(8):
+                summed_columns(k)
+                if k < 4:
+                    hop(k).start()
+        else:
+            loop(n_tp + 1, down, 1)
+
+    def second_hop():
+        if square:
+            for k in range(2):
+                hop(k).wait_recv()
+                t_send[4 + k] = (t_send[4 + k].astype(F32) + t_recv[k].astype(F32)).astype(BF)
+                hop(4 + k).start()
+
+    def give_back():
+        if square:
+            for k in range(2):
+                hop(2 + k).wait_recv()
+                hop(4 + k).wait_recv()
+                out = t_send[6 + k].astype(F32) + t_recv[2 + k].astype(F32) + t_recv[4 + k].astype(F32)
+                e_send[:, :, k * part_w : (k + 1) * part_w] = out.astype(BF).reshape(n_ep, room, part_w)
+        else:
+            out = t_send[t].astype(F32)
+            for d in range(1, n_tp):
+                out = out + t_recv[from_tp(t_recv, ts, tr, d)].astype(F32)
+            e_send[...] = out.astype(BF).reshape(n_ep, room, share)
+        e_recv[ep] = e_send[ep]
+        loop(n_ep, lambda d: to_ep(d).start(), 1)
+
+    def plane_landed(d):
         def beside_landed(s):
-            at = plane(1 + i) * 2 + 1 - core
+            at = source(d) * 2 + 1 - core
             ref = kv_buf.at[at, s]
             remote(ref, ref, lat_own.at[0], lat_recv.at[at * n_tp + s], sibling, t).wait_recv()
 
-        loop(n_tp, beside_landed)
-        project(1 + i)
-        attend_all(False)
-
-    def to_ep(d):
-        to = (ep + d) % n_ep
-        return remote(e_send.at[to], e_recv.at[ep], es.at[d], er.at[ep], to, t)
-
-    def give_back():
-        out = t_send[t].astype(F32)
-        for d in range(1, n_tp):
-            out = out + t_recv[from_tp(t_recv, ts, tr, d)].astype(F32)
-        e_send[...] = out.astype(BF).reshape(n_ep, room, share)
-        e_recv[ep] = e_send[ep]
-        loop(n_ep, lambda d: to_ep(d).start(), 1)
-
-    def tail(i):
-        other(i)
-
-        @pl.when(i == 0)
+        @pl.when(d == 0)
         def _():
-            loop(pieces, projection.relay)
-
-    loop(nz - 1, tail)
-    loop(pieces, projection.last)
+            l_beside.wait_recv()
+
+        @pl.when(d > 0)
+        def _():
+            loop(n_tp, beside_landed)
+
+    def some(count, body, k, of):
+        low, high = count * k // of, count * (k + 1) // of
+        if high > low:
+            loop(high, body, low)
+
+    def lat_push(k, of):
+        some(nz - 1, lambda i: (latents.landed(i, 0), latents.push(i), latents.across(i, 0).start()), k, of)
+
+    def x_push(k, of):
+        some(n_ep - 2, lambda i: (routed.landed(i, 0), routed.push(i)), k, of)
+
+    def x_relay(k, of):
+        some(n_ep - 2, routed.relay, k, of)
+
+    def lat_relay(k, of):
+        some(nz - 1, latents.relay, k, of)
+
+    def lat_last(k, of):
+        some(nz - 1, latents.last, k, of)
+
+    def wo_relay(k, of):
+        some(pieces, projection.relay, k, of)
+
+    def x_last():
+        x_beside.wait_recv()
+        loop(n_ep - 2, routed.last)
+
+    events = [
+        (0, [lambda: x_push(0, 6)]),
+        (1, [lambda: x_push(1, 6)]),
+        (2, [lambda: x_push(2, 6)]),
+        (3, [lambda: x_push(3, 6), lambda: x_relay(0, 6)]),
+        (4, [
+            lambda: x_push(4, 6),
+            lambda: x_relay(1, 6),
+            lambda: x_push(5, 6),
+            lambda: x_relay(2, 6),
+            lambda: x_relay(3, 6),
+            lambda: x_relay(4, 6),
+            lambda: lat_push(0, 3),
+            lambda: x_relay(5, 6),
+            lambda: lat_push(1, 3),
+            lambda: x_last(),
+            lambda: experts_up(),
+            lambda: lat_push(2, 3),
+            lambda: lat_relay(0, 3),
+            lambda: lat_relay(1, 3),
+            lambda: experts_down(),
+            lambda: lat_relay(2, 3),
+            lambda: lat_last(0, 3),
+        ]),
+        (6, [lambda: lat_last(1, 3)]),
+        (8, [
+            lambda: second_hop(),
+            lambda: loop(pieces, projection.push, 1),
+            lambda: wo_relay(0, 4),
+            lambda: lat_last(2, 3),
+        ]),
+        (12, [lambda: wo_relay(1, 4)]),
+        (14, [lambda: wo_relay(2, 4), lambda: give_back()]),
+        (15, [lambda: wo_relay(3, 4)]),
+    ]
+
+    def one(j):
+        for at, todo in events:
+            @pl.when(j == at * beats // 4)
+            def _(todo=todo):
+                for call in todo:
+                    call()
+
+        @pl.when(j % beats == 0)
+        def _():
+            plane_landed(j // beats)
+            project(j // beats)
+
+        beat(j % beats)
+
+    loop(nz * beats, one)
 
     def finish(i):
         here = pl.ds(pl.multiple_of(i * q_block, q_block), q_block)
@@ -502,7 +606,7 @@
 
     loop(n_tp, lambda d: attended(d).start(), 1)
     a_buf[t] = att_ref[piece_of(t), :]
-    give_back()
+    loop(pieces, projection.last)
 
     def across_landed(i):
         def one(d):
@@ -542,7 +646,12 @@
     loop(nz, lambda d: l_to(d).wait_send(), 1)
     loop(nz - 1, lambda i: latents.drain(i, 0))
     loop(pieces, projection.drain)
-    loop(n_tp, lambda d: (term(d).wait_send(), attended(d).wait_send()), 1)
+    if square:
+        for k in range(6):
+            hop(k).wait_send()
+    else:
+        loop(n_tp, lambda d: term(d).wait_send(), 1)
+    loop(n_tp, lambda d: attended(d).wait_send(), 1)
     loop(n_ep, lambda d: to_ep(d).wait_send(), 1)
 
 
@@ -559,7 +668,7 @@
 
 def mega(n_ep, n_tp, heads, operands, w_out, w_gate, w_up, w_down):
     kv, rope, latent = operands[:3]
-    tokens = operands[14]
+    tokens = operands[12]
     rows = latent.shape[0]
     rows_b, width = tokens.shape
     lat = kv.shape[1]
@@ -602,8 +711,8 @@
             pltpu.VMEM((n_ep, room, width), BF),
             pltpu.VMEM((n_ep, room, width), BF),
             pltpu.VMEM((total, hidden), BF),
-            pltpu.VMEM((n_tp, total, share), BF),
-            pltpu.VMEM((n_tp, total, share), BF),
+            pltpu.VMEM((8, total, share // 2) if n_tp == 4 else (n_tp, total, share), BF),
+            pltpu.VMEM((6, total, share // 2) if n_tp == 4 else (n_tp, total, share), BF),
             pltpu.VMEM((n_ep, room, share), BF),
             pltpu.VMEM((n_ep, room, share), BF),
             pltpu.VMEM((rows_b, total), BF),
@@ -624,8 +733,8 @@
             dma((pieces * n_tp,)),
             dma((n_tp,)),
             dma((n_tp,)),
-            dma((n_tp,)),
-            dma((n_tp,)),
+            dma((max(6, n_tp),)),
+            dma((max(6, n_tp),)),
             dma((n_ep,)),
             dma((n_ep,)),
         ],
@@ -664,11 +773,9 @@
     cos_b, sin_b, cos_a, sin_a = turn_tables(n_ep, q_latent.shape[0])
     operands = (
         kv_latent,
-        rope_key,
+        rope_key.T,
         q_latent,
-        q_gain[None, :],
-        kv_gain[None, :],
-        norm_gain_b[None, :],
+        jnp.concatenate([q_gain, kv_gain, norm_gain_b])[None, :],
         cos_b,
         sin_b,
         cos_a,
@@ -678,8 +785,8 @@
         w_k_nope,
         w_value,
         tokens_b,
-        routes,
-        route_logits,
+        routes.T,
+        route_logits.T,
     )
     return mega(n_ep, n_tp, heads, operands, w_out, w_gate[0], w_up[0], w_down[0])
 

time: 91.8 us -> 78.8 us (0.86)
  local copies, waits for them, and re-layouts: 11.6 us -> 4.06 us
  Pallas kernels: 78.7 us -> 72.8 us
    pallas_call x1, Pallas kernels: 78.7 us -> 72.8 us  [mega(): pl.pallas_call(functools.partial(mega_kernel, heads, n_ep, n_tp), out_sha...]
    unnamed x5 -> x2, local copies, waits for them, and re-layouts: 7.78 us -> 3.45 us
    broadcast_in_dim x3 -> x1, local copies, waits for them, and re-layouts: 3.78 us -> 0.61 us  [shards(): jnp.concatenate([q_gain, kv_gain, norm_gain_b])[None, :]]
where the time goes in v2:
time: 78.8 us; the launch traced here: 78.2 us
  Pallas kernels  72.8 us (92%)
  local copies, waits for them, and re-layouts  4.06 us (5%)
    pallas_call x1, Pallas kernels, mega(): pl.pallas_call(functools.partial(mega_kernel, heads, n_ep, n_tp), out_sha...  72.8 us
    unnamed x2, local copies, waits for them, and re-layouts  3.45 us

profile of v2, /device:TPU:0, one launch (start us, length us, event | category | flops | bytes accessed | tf_op | source)
XLA Modules:
  0.0 78.2 jit_solution(16446841002146126434)
XLA Ops:
  0.6 0.7 pad_maximum_fusion
  1.4 0.6 broadcast_in_dim.3.gain_ref
  2.0 72.8 %mega.1 = (bf16[128,2048]{1,0:T(8,128)(2,1)}, bf16[128,512]{1,0:T(8,128)(2,1)}) custom-call(bf16[512,256]{1,0:T(8,128)(2,1)} %kv_ref.1, bf16[32,512]{1,0:T(8,128)(2,1)} %bitcast.9, bf16[512,512]{1,0:T(8,128)(2,1)} %lat_ref.1, bf16[1,2816]{1,0:T(2,128)(2,1)} %broadcast_in_dim.3.gain_ref, f32[512,128]{1,0:T(8,128)} %constant.8.clone.cosb_ref, ...), custom_call_target="tpu_custom_call" | custom-call | flops 13421772800 | bytes 20971520 | tf_op jit(solution)/shard_map/mega/pallas_call | solution.py:689
  74.7 1.9 %copy.25 = bf16[128,2048]{1,0:T(8,128)(2,1)} copy(bf16[128,2048]{1,0:T(8,128)(2,1)} %get-tuple-element.4) | data formatting | bytes 1048576
  76.6 1.6 %copy.26 = bf16[128,512]{1,0:T(8,128)(2,1)} copy(bf16[128,512]{1,0:T(8,128)(2,1)} %get-tuple-element.5) | data formatting | bytes 262144

commit v3 on v2

--- a/solution.py
+++ b/solution.py
@@ -340,9 +340,8 @@
     l_beside.start()
     x_beside.start()
     loop(n_ep - 2, lambda i: x_to(i).start())
-    loop(nz, lambda d: l_to(d).start(), 1)
     loads[0].wait()
-    projection.push(0)
+    loop(pieces // 4, projection.push)
 
     def beside(parts, height, filled):
         filler = jnp.zeros((height, LANES - filled), BF)
@@ -458,11 +457,11 @@
         def _():
             term(d).start()
 
-    def experts_up():
-        loads[1].wait()
-        loads[2].wait()
-        loop(hid.shape[1] // step, up)
-        loads[3].wait()
+    def experts_up(k, of):
+        if k == 0:
+            for load in loads[1:]:
+                load.wait()
+        some(hid.shape[1] // step, up, k, of)
 
     def experts_down():
         if square:
@@ -536,40 +535,42 @@
         x_beside.wait_recv()
         loop(n_ep - 2, routed.last)
 
+    def wo_push(k, of):
+        some(pieces, projection.push, k, of)
+
+    def wo_last(k, of):
+        some(pieces, projection.last, k, of)
+
     events = [
         (0, [lambda: x_push(0, 6)]),
         (1, [lambda: x_push(1, 6)]),
-        (2, [lambda: x_push(2, 6)]),
-        (3, [lambda: x_push(3, 6), lambda: x_relay(0, 6)]),
+        (2, [lambda: x_push(2, 6), lambda: loop(nz, lambda d: l_to(d).start(), 1)]),
+        (3, [lambda: x_push(3, 6), lambda: x_relay(0, 6), lambda: x_relay(1, 6)]),
         (4, [
             lambda: x_push(4, 6),
-            lambda: x_relay(1, 6),
             lambda: x_push(5, 6),
             lambda: x_relay(2, 6),
             lambda: x_relay(3, 6),
             lambda: x_relay(4, 6),
+            lambda: x_relay(5, 6),
             lambda: lat_push(0, 3),
-            lambda: x_relay(5, 6),
             lambda: lat_push(1, 3),
             lambda: x_last(),
-            lambda: experts_up(),
+            lambda: experts_up(0, 2),
             lambda: lat_push(2, 3),
             lambda: lat_relay(0, 3),
             lambda: lat_relay(1, 3),
-            lambda: experts_down(),
+            lambda: experts_up(1, 2),
             lambda: lat_relay(2, 3),
             lambda: lat_last(0, 3),
+            lambda: experts_down(),
         ]),
-        (6, [lambda: lat_last(1, 3)]),
-        (8, [
-            lambda: second_hop(),
-            lambda: loop(pieces, projection.push, 1),
-            lambda: wo_relay(0, 4),
-            lambda: lat_last(2, 3),
-        ]),
-        (12, [lambda: wo_relay(1, 4)]),
-        (14, [lambda: wo_relay(2, 4), lambda: give_back()]),
-        (15, [lambda: wo_relay(3, 4)]),
+        (6, [lambda: second_hop(), lambda: lat_last(1, 3), lambda: loop(pieces, projection.push, 1), lambda: wo_relay(0, 4)]),
+        (9, [lambda: lat_last(2, 3)]),
+        (11, [lambda: give_back(), lambda: wo_relay(1, 4)]),
+        (13, [lambda: wo_relay(2, 4)]),
+        (14, [lambda: wo_relay(3, 4), lambda: wo_last(0, 4)]),
+        (15, [lambda: wo_last(1, 4)]),
     ]
 
     def one(j):
@@ -606,7 +607,8 @@
 
     loop(n_tp, lambda d: attended(d).start(), 1)
     a_buf[t] = att_ref[piece_of(t), :]
-    loop(pieces, projection.last)
+    wo_last(2, 4)
+    wo_last(3, 4)
 
     def across_landed(i):
         def one(d):

time: 78.8 us -> 79.5 us (level)
  Pallas kernels: 72.8 us -> 73.8 us
    pallas_call x1, Pallas kernels: 72.8 us -> 73.8 us  [mega(): pl.pallas_call(functools.partial(mega_kernel, heads, n_ep, n_tp), out_sha...]
where the time goes in v3:
time: 79.5 us; the launch traced here: 79.2 us
  Pallas kernels  73.8 us (93%)
  local copies, waits for them, and re-layouts  4.06 us (5%)
    pallas_call x1, Pallas kernels, mega(): pl.pallas_call(functools.partial(mega_kernel, heads, n_ep, n_tp), out_sha...  73.8 us
    unnamed x2, local copies, waits for them, and re-layouts  3.45 us

profile of v3, /device:TPU:0, one launch (start us, length us, event | category | flops | bytes accessed | tf_op | source)
XLA Modules:
  0.0 79.2 jit_solution(11794867670097002858)
XLA Ops:
  0.6 0.7 pad_maximum_fusion
  1.4 0.6 broadcast_in_dim.3.gain_ref
  2.0 73.8 %mega.1 = (bf16[128,2048]{1,0:T(8,128)(2,1)}, bf16[128,512]{1,0:T(8,128)(2,1)}) custom-call(bf16[512,256]{1,0:T(8,128)(2,1)} %kv_ref.1, bf16[32,512]{1,0:T(8,128)(2,1)} %bitcast.9, bf16[512,512]{1,0:T(8,128)(2,1)} %lat_ref.1, bf16[1,2816]{1,0:T(2,128)(2,1)} %broadcast_in_dim.3.gain_ref, f32[512,128]{1,0:T(8,128)} %constant.8.clone.cosb_ref, ...), custom_call_target="tpu_custom_call" | custom-call | flops 13421772800 | bytes 20971520 | tf_op jit(solution)/shard_map/mega/pallas_call | solution.py:691
  75.8 1.9 %copy.25 = bf16[128,2048]{1,0:T(8,128)(2,1)} copy(bf16[128,2048]{1,0:T(8,128)(2,1)} %get-tuple-element.4) | data formatting | bytes 1048576
  77.7 1.6 %copy.26 = bf16[128,512]{1,0:T(8,128)(2,1)} copy(bf16[128,512]{1,0:T(8,128)(2,1)} %get-tuple-element.5) | data formatting | bytes 262144
